TPU v7x, 128 devices: a whole 4x4x4 slice. The times are simulated.
128 devices in a mesh: sp: 16 (over z, y), tp: 8 (over x, core).
Axes of the slice: x: 4, y: 4, z: 4, core: 2. Of those that a mesh axis runs over, the one named last changes fastest.
Arguments:
- resid: bfloat16 [24576, 2048], P(('sp', 'tp')), may hold values from -6 to 6
- cond: bfloat16 [2048], P('sp'), may hold values from -6 to 6
- mod_shift: bfloat16 [2048, 2048], P('sp', 'tp'), may hold values from -0.125 to 0.125
- mod_scale: bfloat16 [2048, 2048], P('sp', 'tp'), may hold values from -0.125 to 0.125
- mod_gate: bfloat16 [2048, 2048], P('sp', 'tp'), may hold values from -0.125 to 0.125
- norm_gain: float32 [2048], replicated, may hold values from 0.1 to 1.9
- context: bfloat16 [1024, 2048], P('sp'), may hold values from -6 to 6
- w_query: bfloat16 [2048, 2048], P(None, 'tp'), may hold values from -0.125 to 0.125
- w_key: bfloat16 [2048, 2048], P(None, 'tp'), may hold values from -0.125 to 0.125
- w_value: bfloat16 [2048, 2048], P(None, 'tp'), may hold values from -0.125 to 0.125
- query_gain: float32 [128], replicated, may hold values from 0.5 to 6, as said below
- key_gain: float32 [128], replicated, may hold values from 0.5 to 6, as said below
- offset_bias: float32 [16, 15, 31], P('tp'), may hold values from -4 to 4
- context_bias: float32 [16], P('tp'), may hold values from -4.5 to 1
- w_out: bfloat16 [2048, 2048], replicated, may hold values from -0.5 to 0.5
Outputs:
- mixed: bfloat16 [24576, 2048], P(('sp', 'tp'))
Inputs may be any that keep to these rules, and one draw needn't show every extreme that they name: `query_gain`: positive gains. `key_gain`: positive gains.
All inputs are finite; a program needn't handle non-finite values.
Results may differ from a plain program's by a relative error of at most 0.0085.
The roundings to bfloat16 on the way count: a program that leaves them out, or rounds other values in their place, can miss the bound.
Values may be sent and summed in bfloat16 or wider, within the bound.
A program may use at most 128 MiB of HBM per device.

v0:
```python
import functools
import jax
import jax.numpy as jnp
from jax import lax
from jax.sharding import Mesh
from jax.sharding import PartitionSpec as P

HEAD_DIM = 128
GRID_W = 64
WIN_ROWS = 8
WIN_COLS = 16
R_DEV = 24
SP = ("sp_0", "sp_1")
SP_TP = ("sp_0", "sp_1", "tp")
EPS = 1e-06


def over_axes(shard, axes):
    return functools.reduce(lax.psum, axes, shard)


def gather_turned(arrays, axis, dims):
    turned = [jnp.moveaxis(a, dim, 0) for a, dim in zip(arrays, dims)]
    widths = [t[0].size for t in turned]
    both = jnp.concatenate([t.reshape(-1, w) for t, w in zip(turned, widths)], axis=1)
    filled = lax.all_gather(both, axis, axis=0, tiled=True)
    blocks = jnp.split(filled, [sum(widths[:k]) for k in range(1, len(widths))], axis=1)
    return tuple(
        (
            jnp.moveaxis(b.reshape(-1, *t.shape[1:]), 0, dim)
            for b, t, dim in zip(blocks, turned, dims)
        )
    )


def side_by_side(arrays, axis, dim, along):
    both = jnp.concatenate(arrays, axis=along)
    filled, at, done = (lax.all_gather(both, axis, axis=dim, tiled=True), 0, [])
    for a in arrays:
        done.append(lax.slice_in_dim(filled, at, at + a.shape[along], axis=along))
        at += a.shape[along]
    return tuple(done)


def padded_2(cells, sides, width):
    for axis, dim in sides:
        count = lax.axis_size(axis)
        ends = count - 1
        head = lax.slice_in_dim(cells, 0, width, axis=dim)
        tail = lax.slice_in_dim(cells, cells.shape[dim] - width, cells.shape[dim], axis=dim)
        cells = jnp.concatenate(
            [
                lax.ppermute(tail, axis, [(i, (i + 1) % count) for i in range(ends)]),
                cells,
                lax.ppermute(head, axis, [((i + 1) % count, i) for i in range(ends)]),
            ],
            axis=dim,
        )
    return cells


def head_norm(values, gain, heads_local):
    count = values.shape[0]
    split = values.reshape(count, heads_local, -1)
    scaled = split * lax.rsqrt(jnp.mean(split * split, axis=-1, keepdims=True) + EPS) * gain
    return scaled.reshape(count, -1).astype(jnp.bfloat16)


def project_context(rows_in, norm_gain, w_key, w_value, key_gain, heads_local):
    floats = rows_in.astype(jnp.float32)
    inverse = lax.rsqrt(jnp.mean(floats * floats, axis=-1, keepdims=True) + EPS)
    normed = (floats * inverse * norm_gain).astype(jnp.bfloat16)
    keys = head_norm(
        jnp.dot(normed, w_key, preferred_element_type=jnp.float32), key_gain, heads_local
    )
    values = jnp.dot(normed, w_value, preferred_element_type=jnp.float32).astype(jnp.bfloat16)
    return (keys, values)


def attend_rows(
    queries, key_at, value_at, row_offset, offset_bias, ctx_key, ctx_value, context_bias
):
    grid_w = queries.shape[1]
    columns = jnp.arange(grid_w, dtype=jnp.int32)
    col_begin = jnp.clip(columns - WIN_COLS // 2, 0, grid_w - WIN_COLS)
    valid = (columns[None, :] >= col_begin[:, None]) & (
        columns[None, :] < col_begin[:, None] + WIN_COLS
    )
    col_offset = jnp.clip(columns[None, :] - columns[:, None] + WIN_COLS - 1, 0, 2 * WIN_COLS - 2)
    col_onehot = (col_offset[..., None] == jnp.arange(2 * WIN_COLS - 1, dtype=jnp.int32)).astype(
        jnp.float32
    )
    row_onehot = (
        row_offset[:, :, None] == jnp.arange(2 * WIN_ROWS - 1, dtype=jnp.int32)[None, None, :]
    ).astype(jnp.float32)
    bias = jnp.einsum(
        "nir,hrj,ckj->nhcik", row_onehot, offset_bias, col_onehot, precision=lax.Precision.HIGHEST
    )
    factor = HEAD_DIM ** (-0.5)
    s_win = (
        jnp.stack(
            [
                jnp.einsum(
                    "nchd,nkhd->nhck", queries, key_at(i), preferred_element_type=jnp.float32
                )
                for i in range(WIN_ROWS)
            ],
            axis=3,
        )
        * factor
        + bias
    )
    s_win = jnp.where(valid[None, None, :, None, :], s_win, -1e30)
    s_ctx = (
        jnp.einsum("nchd,jhd->nhcj", queries, ctx_key, preferred_element_type=jnp.float32) * factor
    )
    s_ctx = s_ctx + context_bias[None, :, None, None]
    top = jnp.maximum(jnp.max(s_win, axis=(3, 4)), jnp.max(s_ctx, axis=3))
    e_win = jnp.exp(s_win - top[..., None, None])
    e_ctx = jnp.exp(s_ctx - top[..., None])
    total = jnp.sum(e_win, axis=(3, 4)) + jnp.sum(e_ctx, axis=3)
    p_win = (e_win / total[..., None, None]).astype(jnp.bfloat16)
    p_ctx = (e_ctx / total[..., None]).astype(jnp.bfloat16)
    out = jnp.einsum("nhcj,jhd->nchd", p_ctx, ctx_value, preferred_element_type=jnp.float32)
    for i in range(WIN_ROWS):
        out = out + jnp.einsum(
            "nhck,nkhd->nchd", p_win[:, :, :, i], value_at(i), preferred_element_type=jnp.float32
        )
    count = queries.shape[0]
    return out.astype(jnp.bfloat16).reshape(count * grid_w, -1)


def shards(
    resid,
    cond,
    mod_shift,
    mod_scale,
    mod_gate,
    norm_gain,
    context,
    w_query,
    w_key,
    w_value,
    query_gain,
    key_gain,
    offset_bias,
    context_bias,
    w_out,
):
    heads_local = offset_bias.shape[0]
    width = w_query.shape[1]
    lifted = jax.nn.silu(cond.astype(jnp.float32)).astype(jnp.bfloat16)
    shift_part = jnp.dot(lifted, mod_shift, preferred_element_type=jnp.float32)
    scale_part = jnp.dot(lifted, mod_scale, preferred_element_type=jnp.float32)
    gate_part = jnp.dot(lifted, mod_gate, preferred_element_type=jnp.float32)
    summed = (over_axes(shift_part, SP), over_axes(scale_part, SP), over_axes(gate_part, SP))
    shift, scale, gate = gather_turned((summed[0], summed[1], summed[2]), "tp", (0, 0, 0))
    floats = resid.astype(jnp.float32)
    inverse = lax.rsqrt(jnp.mean(floats * floats, axis=-1, keepdims=True) + EPS)
    normed = (floats * inverse * norm_gain * (1.0 + scale) + shift).astype(jnp.bfloat16)
    piece = lax.all_gather(normed, "tp", axis=0, tiled=True)
    queries = head_norm(
        jnp.dot(piece, w_query, preferred_element_type=jnp.float32), query_gain, heads_local
    )
    keys = head_norm(
        jnp.dot(piece, w_key, preferred_element_type=jnp.float32), key_gain, heads_local
    )
    values = jnp.dot(piece, w_value, preferred_element_type=jnp.float32).astype(jnp.bfloat16)
    projected = jnp.concatenate([queries, keys, values], axis=1)
    query = projected[:, :width]
    key_value = projected[:, width:]
    own_key, own_value = project_context(context, norm_gain, w_key, w_value, key_gain, heads_local)
    ctx_key, ctx_value = side_by_side((own_key, own_value), SP, 0, 1)
    ctx_count = ctx_key.shape[0]
    ctx_key = ctx_key.reshape(ctx_count, heads_local, HEAD_DIM)
    ctx_value = ctx_value.reshape(ctx_count, heads_local, HEAD_DIM)
    reach = WIN_ROWS // 2
    grid = key_value.reshape(R_DEV, GRID_W, 2 * width)
    padded = padded_2(grid, ((SP, 0),), reach)
    padded = padded.reshape(R_DEV + 2 * reach, GRID_W, 2, heads_local, HEAD_DIM)
    total_rows = R_DEV * lax.axis_size(SP)
    first = lax.axis_index(SP) * R_DEV
    global_rows = first + jnp.arange(R_DEV, dtype=jnp.int32)
    row_start = jnp.clip(global_rows - reach, 0, total_rows - WIN_ROWS)
    window_rows = jnp.arange(WIN_ROWS, dtype=jnp.int32)[None, :]
    row_offset = row_start[:, None] + window_rows - global_rows[:, None] + WIN_ROWS - 1
    queries = query.reshape(R_DEV, GRID_W, heads_local, HEAD_DIM)
    upper = min(reach, R_DEV)
    lower = max(upper, R_DEV - reach)
    edge_rows = list(range(upper)) + list(range(lower, R_DEV))
    edge_index = jnp.array(edge_rows, dtype=jnp.int32)
    edge_window = (jnp.take(row_start, edge_index) - first + reach)[:, None] + window_rows
    edge_kv = jnp.take(padded, edge_window, axis=0)
    edge_out = attend_rows(
        jnp.take(queries, edge_index, axis=0),
        lambda i: edge_kv[:, i, :, 0],
        lambda i: edge_kv[:, i, :, 1],
        jnp.take(row_offset, edge_index, axis=0),
        offset_bias,
        ctx_key,
        ctx_value,
        context_bias,
    )
    pieces = [edge_out[: upper * GRID_W]]
    middle = lower - upper
    inner_out = attend_rows(
        queries[upper:lower],
        lambda i: padded[upper + i : upper + i + middle, :, 0],
        lambda i: padded[upper + i : upper + i + middle, :, 1],
        row_offset[upper:lower],
        offset_bias,
        ctx_key,
        ctx_value,
        context_bias,
    )
    pieces.append(inner_out)
    pieces.append(edge_out[upper * GRID_W :])
    attended = jnp.concatenate(pieces, axis=0)
    full_rows = lax.all_to_all(attended, "tp", split_axis=0, concat_axis=1, tiled=True)
    result = jnp.dot(full_rows, w_out, preferred_element_type=jnp.float32)
    return (floats + gate * result).astype(jnp.bfloat16)


def solution(mesh):
    split = Mesh(mesh.devices.reshape(4, 4, mesh.shape["tp"]), ("sp_0", "sp_1", "tp"))
    placed = (
        P(SP_TP, None),
        P(SP),
        P(SP, "tp"),
        P(SP, "tp"),
        P(SP, "tp"),
        P(),
        P(SP, None),
        P(None, "tp"),
        P(None, "tp"),
        P(None, "tp"),
        P(),
        P(),
        P("tp", None, None),
        P("tp"),
        P(),
    )
    return jax.shard_map(
        shards, mesh=split, in_specs=placed, out_specs=P(SP_TP, None), check_vma=False
    )
```

profile of v0, /device:TPU:24, one launch (start us, length us, event | category | flops | bytes accessed | tf_op | source)
XLA Modules:
  0.0 245.6 jit_solution(12134459745243298402)
XLA Ops:
  15.5 11.7 %all-reduce.1 = (f32[256]{0:T(256)S(1)}, f32[256]{0:T(256)S(1)}, f32[256]{0:T(256)S(1)}) all-reduce(f32[256]{0:T(256)S(1)} %bitcast.451, f32[256]{0:T(256)S(1)} %bitcast.450, f32[256]{0:T(256)S(1)} %bitcast.449), channel_id=1, replica_groups=mesh['sp_0'=4,'sp_1'=4,'tp'=8] {'sp_0'}, use_global_device_ids=true, to_apply=%region_4.5 | all-reduce | flops 768 | bytes 6144 | tf_op jit(solution)/shard_map/psum | solution.py:19
  27.3 7.5 %all-reduce = (f32[256,1]{0,1:T(1,128)S(1)}, f32[256,1]{0,1:T(1,128)S(1)}, f32[256,1]{0,1:T(1,128)S(1)}) all-reduce(f32[256,1]{0,1:T(1,128)S(1)} %bitcast.452, f32[256,1]{0,1:T(1,128)S(1)} %bitcast.453, f32[256,1]{0,1:T(1,128)S(1)} %bitcast.454), channel_id=1, replica_groups=mesh['sp_0'=4,'sp_1'=4,'tp'=8] {'sp_1'}, use_global_device_ids=true, to_apply=%region_5.6 | all-reduce | flops 768 | bytes 6144 | tf_op jit(solution)/shard_map/psum | solution.py:19
  34.7 13.3 %all_gather.9 = f32[2048,3]{0,1:T(4,128)S(1)} all-gather(f32[256,3]{0,1:T(4,128)S(1)} %pad_maximum_fusion.4), channel_id=1, replica_groups=mesh['sp_0'=4,'sp_1'=4,'tp'=8] {'tp'}, dimensions={0}, use_global_device_ids=true | all-gather | bytes 27648 | tf_op jit(solution)/shard_map/all_gather | solution.py:26
  51.6 6.1 %fusion.111 = f32[64,64,2,16,8]{1,3,4,2,0:T(8,128)} fusion(f32[64,64,2,15,1]{1,3,4,2,0:T(8,128)S(1)} %convolution_bitcast_fusion.16, s32[16,8]{0,1:T(8,128)S(1)} %copy.538), kind=kOutput, calls=%fused_computation.234 | convolution fusion | flops 188745600 | bytes 4686336 | tf_op jit(solution)/shard_map/nir,hrj,ckj->nhcik/dot_general | solution.py:96
  57.7 9.6 %copy.539 = f32[64,64,2,16,8]{0,1,2,3,4:T(8,128)} copy(f32[64,64,2,16,8]{1,3,4,2,0:T(8,128)} %fusion.111) | data formatting | bytes 8388608 | tf_op jit(solution)/shard_map/nir,hrj,ckj->nhcik/dot_general | solution.py:96
  67.5 3.8 %fusion.116 = f32[64,64,2,8,8]{1,4,3,2,0:T(8,128)} fusion(f32[64,64,2,15,1]{1,3,4,2,0:T(8,128)S(1)} %convolution_bitcast_fusion.16, s32[8,8]{1,0:T(8,128)S(1)} %gather_fusion.3), kind=kOutput, calls=%fused_computation.243 | convolution fusion | flops 94372800 | bytes 2588928 | tf_op jit(solution)/shard_map/nir,hrj,ckj->nhcik/dot_general | solution.py:96
  71.3 5.6 %copy.496 = f32[64,64,2,8,8]{0,1,2,3,4:T(8,128)} copy(f32[64,64,2,8,8]{1,4,3,2,0:T(8,128)} %fusion.116) | data formatting | bytes 4194304 | tf_op jit(solution)/shard_map/nir,hrj,ckj->nhcik/dot_general | solution.py:96
  80.1 19.1 %all-gather.5.cloned.1.call-done = bf16[1536,2048]{1,0:T(8,128)(2,1)} async-done(((bf16[192,2048]{1,0:T(8,128)(2,1)}), bf16[1536,2048]{1,0:T(8,128)(2,1)}) %all-gather.5.cloned.1.call-update) | async-done | bytes 6291472 | tf_op jit(solution)/shard_map/all_gather | solution.py:161
  99.2 4.8 %bitcast_reduce_fusion.2 = (f32[1536,2]{0,1:T(2,128)S(1)}, f32[1536,256]{0,1:T(8,128)S(1)}) fusion(bf16[1536,2048]{1,0:T(8,128)(2,1)} %all-gather.5.cloned.1.call-done, bf16[2048,256]{1,0:T(8,128)(2,1)S(1)} %copy-done), kind=kOutput, calls=%fused_computation.49 | convolution fusion | flops 1611396096 | bytes 8925184 | tf_op jit(solution)/shard_map/dot_general | solution.py:166
  110.3 8.0 %fusion.139 = (bf16[16,64,1,2,128]{4,3,2,1,0:T(2,128)(2,1)}, bf16[16,64,1,2,128]{4,3,2,1,0:T(2,128)(2,1)}, bf16[16,64,1,2,128]{4,3,2,1,0:T(2,128)(2,1)}, bf16[16...) fusion(bf16[24,64,2,2,128]{4,3,2,1,0:T(2,128)(2,1)S(1)} %concat, ...), kind=kLoop, calls=%fused_computation.286 | loop fusion | bytes 16777216 | tf_op jit(solution)/shard_map/slice | solution.py:209
  118.3 4.7 %bitcast_reduce_fusion.3 = (f32[1536,2]{0,1:T(2,128)S(1)}, f32[1536,256]{0,1:T(8,128)S(1)}) fusion(bf16[1536,2048]{1,0:T(8,128)(2,1)} %all-gather.5.cloned.1.call-done, bf16[2048,256]{1,0:T(8,128)(2,1)S(1)} %copy-done.41), kind=kOutput, calls=%fused_computation.53 | convolution fusion | flops 1611396096 | bytes 8925184 | tf_op jit(solution)/shard_map/dot_general | solution.py:163
  133.1 3.3 %copy-done.7 = f32[16,2,64,8,64]{2,4,1,0,3:T(8,128)} copy-done((f32[16,2,64,8,64]{2,4,1,0,3:T(8,128)}, f32[16,2,64,8,64]{2,4,1,0,3:T(8,128)S(1)}, u32[]{:S(2)}) %copy-start.7) | copy-done | bytes 4194328
  137.7 3.2 %copy-done.2 = f32[2,1024,1024]{1,2,0} copy-done((f32[2,1024,1024]{1,2,0}, f32[2,1024,1024]{1,2,0:S(1)}, u32[]{:S(2)}) %copy-start.2) | copy-done | bytes 8388632
  141.8 12.2 %fusion.135 = (f32[16,2,64]{2,1,0:T(2,128)S(1)}, f32[16,2,64,8,64]{2,4,1,0,3:T(8,128)}) fusion(f32[64,64,2,16,8]{0,1,2,3,4:T(8,128)} %copy.539, f32[16,2,64,8,64]{2,4,1,0,3:T(8,128)} %copy-done.7, pred[64,64]{0,1:T(8,128)(4,1)S(1)} %fusion.114), kind=kLoop, calls=%fused_computation.284 | loop fusion | flops 4192256 | bytes 12595200 | tf_op jit(solution)/shard_map/reduce_max | solution.py:118
  154.1 4.5 %fusion.3 = f32[16,2,64]{2,0,1:T(8,128)S(1)} fusion(f32[2,1024,16,64]{1,3,2,0:T(8,128)} %bitcast.426, f32[16,2,64]{2,0,1:T(8,128)S(1)} %copy_maximum_fusion, f32[2]{0:T(128)S(1)} %copy-done.38), kind=kLoop, calls=%fused_computation.14 | loop fusion | flops 8386560 | bytes 8405000 | tf_op jit(solution)/shard_map/reduce_sum | solution.py:121
  162.3 4.8 %fusion.2 = f32[16,2,64]{2,1,0:T(2,128)S(1)} fusion(f32[16,2,64,8,64]{2,4,1,0,3:T(8,128)} %get-tuple-element.12, f32[16,2,64]{2,1,0:T(2,128)S(1)} %copy.541), kind=kLoop, calls=%fused_computation.13 | loop fusion | flops 2095104 | bytes 4210688 | tf_op jit(solution)/shard_map/reduce_sum | solution.py:121
  167.1 4.3 %divide_convert_fusion = bf16[16,2,64,8,64]{2,4,1,0,3:T(8,128)(2,1)S(1)} fusion(f32[16,2,64,8,64]{2,4,1,0,3:T(8,128)} %get-tuple-element.12, f32[16,2,64]{2,1,0:T(2,128)S(1)} %copy.545, f32[16,2,64]{2,1,0:T(2,128)S(1)} %copy.541), kind=kLoop, calls=%fused_computation.9 | loop fusion | flops 3145728 | bytes 6307840 | tf_op jit(solution)/shard_map/convert_element_type | solution.py:122
  182.5 3.4 %collective-permute-start = (bf16[4,64,512]{2,1,0:T(8,128)(2,1)}, bf16[4,64,512]{2,1,0:T(8,128)(2,1)}, u32[]{:S(2)}, u32[]{:S(2)}) collective-permute-start(bf16[4,64,512]{2,1,0:T(8,128)(2,1)} %bitcast.23), channel_id=1, source_target_pairs={{0,8},{8,16},{16,24},{24,32},{32,40},{40,48},{48,56},{56,64},{64,7... | collective-permute-start | bytes 786440 | tf_op jit(solution)/shard_map/ppermute | solution.py:53
  186.8 2.4 collective-permute-start.1
  195.4 3.9 %collective-permute-done.1 = bf16[4,64,512]{2,1,0:T(8,128)(2,1)} collective-permute-done((bf16[4,64,512]{2,1,0:T(8,128)(2,1)}, bf16[4,64,512]{2,1,0:T(8,128)(2,1)}, u32[]{:S(2)}, u32[]{:S(2)}) %collective-permute-start.1) | collective-permute-done | bytes 262176 | tf_op jit(solution)/shard_map/ppermute | solution.py:55
  202.0 3.1 %gather_fusion.2 = bf16[64,64,2,2,128]{4,1,3,2,0:T(8,128)(2,1)} fusion(bf16[32,64,2,2,128]{4,1,3,2,0:T(8,128)(2,1)S(1)} %pad_maximum_fusion, s32[1024]{0:T(1024)S(1)} %pad_clamp_fusion), kind=kCustom, calls=%fused_computation.2 | custom fusion | bytes 8388864 | tf_op jit(solution)/shard_map/jit(_take)/gather | solution.py:193
  205.1 2.6 %copy_select_fusion = bf16[8,8,64,2,2,128]{5,2,4,0,3,1:T(8,128)(2,1)S(1)} fusion(bf16[8,8,64,2,2,128]{5,2,4,3,1,0:T(8,128)(2,1)} %bitcast.431, pred[8,8]{0,1:T(8,128)(4,1)S(1)} %fusion.123), kind=kLoop, calls=%fused_computation.20 | loop fusion | flops 2097152 | bytes 8388672 | tf_op jit(solution)/shard_map/jit(_take)/select_n | solution.py:193
  219.5 16.2 %all_to_all.19 = bf16[8,192,256]{2,1,0:T(8,128)(2,1)S(1)} all-to-all(bf16[8,192,256]{2,1,0:T(8,128)(2,1)S(1)} %bitcast.432), channel_id=1, replica_groups=mesh['sp_0'=4,'sp_1'=4,'tp'=8] {'tp'}, dimensions={0} | all-to-all | bytes 1572864 | tf_op jit(solution)/shard_map/all_to_all | solution.py:219
  235.8 2.7 %fusion.10 = bf16[192,2048]{1,0:T(8,128)(2,1)} fusion(bf16[192,2048]{1,0:T(8,128)(2,1)S(1)} %bitcast.438, bf16[2048,2048]{1,0:T(8,128)(2,1)S(1)} %bitcast.456, bf16[192,2048]{1,0:T(8,128)(2,1)S(1)} %copy-done.13, f32[2048]{0:T(1024)S(1)} %bitcast.448), kind=kOutput, calls=%fused_computation.31 | convolution fusion | flops 1612185600 | bytes 10756096 | tf_op jit(solution)/shard_map/dot_general | solution.py:220
  (220 shorter events, 70.0 us)
Async XLA Ops:
  6.5 43.1 %copy-start.39 = (s32[8]{0:T(128)S(1)}, s32[8]{0:T(128)}, u32[]{:S(2)}) copy-start(s32[8]{0:T(128)} %constant.138) | copy-start | bytes 100
  6.5 41.7 %copy-start.36 = (f32[2048]{0:T(1024)S(1)}, f32[2048]{0:T(1024)}, u32[]{:S(2)}) copy-start(f32[2048]{0:T(1024)} %param.21) | copy-start | bytes 24580
  6.5 41.5 %copy-start.12 = (bf16[192,2048]{1,0:T(8,128)(2,1)S(1)}, bf16[192,2048]{1,0:T(8,128)(2,1)}, u32[]{:S(2)}) copy-start(bf16[192,2048]{1,0:T(8,128)(2,1)} %param.16) | copy-start | bytes 2359300
  6.5 44.4 %copy-start.37 = (f32[2,15,31]{2,0,1:T(2,128)S(1)}, f32[2,15,31]{2,0,1:T(2,128)}, u32[]{:S(2)}) copy-start(f32[2,15,31]{2,0,1:T(2,128)} %param.28) | copy-start | bytes 11164
  6.5 70.4 %all-gather.3.cloned.1.call-start = ((), (), s32[]{:S(2)}) async-start(), calls=%async_computation.1 | async-start | bytes 1114112 | tf_op jit(solution)/shard_map/all_gather | solution.py:38
  12.5 86.7 %all-gather.5.cloned.1.call-start = ((), (), s32[]{:S(2)}) async-start(), calls=%async_computation.2 | async-start | bytes 7077888 | tf_op jit(solution)/shard_map/all_gather | solution.py:161
  71.3 5.6 %copy-start.42 = (f32[128]{0:T(128)S(1)}, f32[128]{0:T(128)}, u32[]{:S(2)}) copy-start(f32[128]{0:T(128)} %param.26) | copy-start | bytes 1540
  80.1 24.1 %copy-start.31 = (bf16[2048,256]{1,0:T(8,128)(2,1)S(1)}, bf16[2048,256]{1,0:T(8,128)(2,1)}, u32[]{:S(2)}) copy-start(bf16[2048,256]{1,0:T(8,128)(2,1)} %param.25) | copy-start | bytes 3145732
  99.2 5.0 %copy-start.40 = (bf16[1536,2048]{1,0:T(8,128)(2,1)S(1)}, bf16[1536,2048]{1,0:T(8,128)(2,1)}, u32[]{:S(2)}) copy-start(bf16[1536,2048]{1,0:T(8,128)(2,1)} %all-gather.5.cloned.1.call-done) | copy-start | bytes 18874372
  106.2 4.1 %copy-start.14 = (bf16[1536,256]{0,1:T(8,128)(2,1)}, bf16[1536,256]{0,1:T(8,128)(2,1)S(1)}, u32[]{:S(2)}) copy-start(bf16[1536,256]{0,1:T(8,128)(2,1)S(1)} %convolution_convert_fusion) | copy-start | bytes 2359300
  110.2 8.0 %copy-start.41 = (bf16[2048,256]{1,0:T(8,128)(2,1)S(1)}, bf16[2048,256]{1,0:T(8,128)(2,1)}, u32[]{:S(2)}) copy-start(bf16[2048,256]{1,0:T(8,128)(2,1)} %param.23) | copy-start | bytes 3145732
  126.3 4.8 %copy-start.29 = (bf16[16,64,1,2,128]{4,3,2,1,0:T(2,128)(2,1)S(1)}, bf16[16,64,1,2,128]{4,3,2,1,0:T(2,128)(2,1)}, u32[]{:S(2)}) copy-start(bf16[16,64,1,2,128]{4,3,2,1,0:T(2,128)(2,1)} %get-tuple-element.50) | copy-start | bytes 1572868
  127.6 3.8 %copy-start.28 = (bf16[16,64,1,2,128]{4,3,2,1,0:T(2,128)(2,1)S(1)}, bf16[16,64,1,2,128]{4,3,2,1,0:T(2,128)(2,1)}, u32[]{:S(2)}) copy-start(bf16[16,64,1,2,128]{4,3,2,1,0:T(2,128)(2,1)} %get-tuple-element.49) | copy-start | bytes 1572868
  131.5 4.9 %copy-start.10 = (bf16[128,2,8,128]{3,2,1,0:T(8,128)(2,1)S(1)}, bf16[128,2,8,128]{3,2,1,0:T(8,128)(2,1)}, u32[]{:S(2)}) copy-start(bf16[128,2,8,128]{3,2,1,0:T(8,128)(2,1)} %get-tuple-element.58) | copy-start | bytes 1572868
  136.4 4.5 %copy-start.38 = (f32[2]{0:T(128)S(1)}, f32[2]{0:T(128)}, u32[]{:S(2)}) copy-start(f32[2]{0:T(128)} %param.29) | copy-start | bytes 28
  154.1 6.2 %copy-start.15 = (bf16[1536,256]{0,1:T(8,128)(2,1)S(1)}, bf16[1536,256]{0,1:T(8,128)(2,1)}, u32[]{:S(2)}) copy-start(bf16[1536,256]{0,1:T(8,128)(2,1)} %copy-done.14) | copy-start | bytes 2359300
  167.1 6.2 %copy-start.34 = (bf16[1024,2,128]{2,1,0:T(2,128)(2,1)S(1)}, bf16[1024,2,128]{2,1,0:T(2,128)(2,1)}, u32[]{:S(2)}) copy-start(bf16[1024,2,128]{2,1,0:T(2,128)(2,1)} %reshape.300) | copy-start | bytes 1572868
  179.5 6.4 %copy-start.32 = (bf16[256,512]{0,1:T(8,128)(2,1)S(1)}, bf16[256,512]{0,1:T(8,128)(2,1)}, u32[]{:S(2)}) copy-start(bf16[256,512]{0,1:T(8,128)(2,1)} %get-tuple-element.56) | copy-start | bytes 786436
  179.9 11.2 %copy-start.11 = (bf16[128,2,8,128]{3,2,1,0:T(8,128)(2,1)S(1)}, bf16[128,2,8,128]{3,2,1,0:T(8,128)(2,1)}, u32[]{:S(2)}) copy-start(bf16[128,2,8,128]{3,2,1,0:T(8,128)(2,1)} %get-tuple-element.58) | copy-start | bytes 1572868
  182.5 11.8 %collective-permute-start = (bf16[4,64,512]{2,1,0:T(8,128)(2,1)}, bf16[4,64,512]{2,1,0:T(8,128)(2,1)}, u32[]{:S(2)}, u32[]{:S(2)}) collective-permute-start(bf16[4,64,512]{2,1,0:T(8,128)(2,1)} %bitcast.23), channel_id=1, source_target_pairs={{0,8},{8,16},{16,24},{24,32},{32,40},{40,48},{48,56},{56,64},{64,7... | collective-permute-start | bytes 786440 | tf_op jit(solution)/shard_map/ppermute | solution.py:53
  186.8 12.5 %collective-permute-start.1 = (bf16[4,64,512]{2,1,0:T(8,128)(2,1)}, bf16[4,64,512]{2,1,0:T(8,128)(2,1)}, u32[]{:S(2)}, u32[]{:S(2)}) collective-permute-start(bf16[4,64,512]{2,1,0:T(8,128)(2,1)} %bitcast.24), channel_id=1, source_target_pairs={{8,0},{16,8},{24,16},{32,24},{40,32},{48,40},{56,48},{64,56},{72,6... | collective-permute-start | bytes 786440 | tf_op jit(solution)/shard_map/ppermute | solution.py:55
  216.3 19.4 %slice-start = ((s8[8388608]{0:T(1024)(128)(4,1)}), s8[4194304]{0:T(1024)(128)(4,1)S(1)}, s32[]{:S(2)}) async-start(s8[8388608]{0:T(1024)(128)(4,1)} %bitcast.455), calls=%async_computation.3 | async-start | bytes 8388608
  218.2 17.5 %slice-start.1 = ((s8[8388608]{0:T(1024)(128)(4,1)}), s8[4194304]{0:T(1024)(128)(4,1)S(1)}, s32[]{:S(2)}) async-start(s8[8388608]{0:T(1024)(128)(4,1)} %bitcast.455), calls=%async_computation.4 | async-start | bytes 8388608
  219.0 16.7 %copy-start.13 = (bf16[192,2048]{1,0:T(8,128)(2,1)S(1)}, bf16[192,2048]{1,0:T(8,128)(2,1)}, u32[]{:S(2)}) copy-start(bf16[192,2048]{1,0:T(8,128)(2,1)} %param.16) | copy-start | bytes 2359300
  (25 other events, 51.1 us)
Sparse Core Ops, SparseCore 0:
  12.6 44.4 all-gather.2
  58.8 40.3 all-gather.4
where the time goes:
time: 250 us; the launch traced here: 246 us
  local copies, waits for them, and re-layouts  63.7 us (25%)
  matrix products  48.7 us (19%)
  blocking collectives  48.6 us (19%)
  other arithmetic  40.8 us (16%)
  waiting for transfers between devices  23 us (9%)
  between operations  14.8 us (6%)
  starting transfers between devices  5.9 us (2%)
    psum x2, blocking collectives, over_axes(): return functools.reduce(lax.psum, axes, shard)  19.2 us
    all_gather x1, waiting for transfers between devices, shards(): piece = lax.all_gather(normed, 'tp', axis=0, tiled=True)  19.1 us
    all_to_all x1, blocking collectives, shards(): lax.all_to_all(attended, 'tp', split_axis=0, concat_axis=1, tiled=True)  16.2 us
    reduce_max x4, other arithmetic, attend_rows(): top = jnp.maximum(jnp.max(s_win, axis=(3, 4)), jnp.max(s_ctx, axis=3))  15.3 us
    dot_general x2, local copies, waits for them, and re-layouts, attend_rows(): jnp.einsum('nir,hrj,ckj->nhcik', row_onehot, offset_bias, col_onehot, pre...  15.2 us
    all_gather x1, blocking collectives, gather_turned(): filled = lax.all_gather(both, axis, axis=0, tiled=True)  13.3 us
    unnamed x93, local copies, waits for them, and re-layouts  12 us
    reduce_sum x4, other arithmetic, attend_rows(): total = jnp.sum(e_win, axis=(3, 4)) + jnp.sum(e_ctx, axis=3)  11 us
  transfers between devices with their start and end apart: 4, of which 2 were waited for; matrix products, arithmetic and copies ran while one was open for 16% of the time, Pallas kernels for 0%

commit v1 on v0

--- a/solution.py
+++ b/solution.py
@@ -158,7 +158,9 @@
     floats = resid.astype(jnp.float32)
     inverse = lax.rsqrt(jnp.mean(floats * floats, axis=-1, keepdims=True) + EPS)
     normed = (floats * inverse * norm_gain * (1.0 + scale) + shift).astype(jnp.bfloat16)
-    piece = lax.all_gather(normed, "tp", axis=0, tiled=True)
+    piece = jnp.concatenate(
+        lax.all_to_all(jnp.stack([normed] * lax.axis_size("tp")), "tp", 0, 0), axis=0
+    )
     queries = head_norm(
         jnp.dot(piece, w_query, preferred_element_type=jnp.float32), query_gain, heads_local
     )

time: 250 us -> 269 us (1.076)
  waiting for transfers between devices: 23 us -> 40.3 us
  matrix products: 48.7 us -> 58.3 us
  other arithmetic: 40.8 us -> 34.6 us
  local copies, waits for them, and re-layouts: 63.7 us -> 58.1 us
  starting transfers between devices: 5.9 us -> 11.1 us
    all_to_all x0 -> x1, waiting for transfers between devices: none -> 23.6 us  [shards(): lax.all_to_all(jnp.stack([normed] * lax.axis_size('tp')), 'tp', 0, 0)]
    all_gather x1 -> x0, waiting for transfers between devices: 19.1 us -> none  [shards(): piece = lax.all_gather(normed, 'tp', axis=0, tiled=True)]
    all_gather x1, waiting for transfers between devices: 0.02 us -> 12.4 us  [side_by_side(): filled, at, done = (lax.all_gather(both, axis, axis=dim, tiled=True), 0, [])]
    dot_general x1, matrix products: 4.67 us -> 16.5 us  [shards(): jnp.dot(piece, w_query, preferred_element_type=jnp.float32)]
    all_to_all x0 -> x1, starting transfers between devices: none -> 4.89 us  [shards(): lax.all_to_all(jnp.stack([normed] * lax.axis_size('tp')), 'tp', 0, 0)]
    slice x4 -> x1, local copies, waits for them, and re-layouts: 4.32 us -> 0.04 us  [shards(): queries[upper:lower]]
    dot_general x0 -> x2, local copies, waits for them, and re-layouts: none -> 4.09 us  [the longest x1 2.3 us: shards(): jnp.dot(piece, w_query, preferred_element_type=jnp.float32)]
    another operation x0 -> x1, local copies, waits for them, and re-layouts: none -> 3.47 us  [shards(): jnp.stack([normed] * lax.axis_size('tp'))]
  transfers between devices with their start and end apart: 4 -> 4, of which waited for: 2 -> 3; matrix products, arithmetic and copies ran while one was open for 16% -> 15% of each run, Pallas kernels for 0% -> 0%
where the time goes in v1:
time: 269 us; the launch traced here: 265 us
  matrix products  58.3 us (22%)
  local copies, waits for them, and re-layouts  58.1 us (22%)
  blocking collectives  48.2 us (18%)
  waiting for transfers between devices  40.3 us (15%)
  other arithmetic  34.6 us (13%)
  between operations  14.6 us (5%)
  starting transfers between devices  11.1 us (4%)
    all_to_all x1, waiting for transfers between devices, shards(): lax.all_to_all(jnp.stack([normed] * lax.axis_size('tp')), 'tp', 0, 0)  23.6 us
    psum x2, blocking collectives, over_axes(): return functools.reduce(lax.psum, axes, shard)  19.2 us
    dot_general x1, matrix products, shards(): jnp.dot(piece, w_query, preferred_element_type=jnp.float32)  16.5 us
    all_to_all x1, blocking collectives, shards(): lax.all_to_all(attended, 'tp', split_axis=0, concat_axis=1, tiled=True)  15.7 us
    dot_general x2, local copies, waits for them, and re-layouts, attend_rows(): jnp.einsum('nir,hrj,ckj->nhcik', row_onehot, offset_bias, col_onehot, pre...  15.3 us
    reduce_max x4, other arithmetic, attend_rows(): top = jnp.maximum(jnp.max(s_win, axis=(3, 4)), jnp.max(s_ctx, axis=3))  15.2 us
    all_gather x1, blocking collectives, gather_turned(): filled = lax.all_gather(both, axis, axis=0, tiled=True)  13.3 us
    all_gather x1, waiting for transfers between devices, side_by_side(): filled, at, done = (lax.all_gather(both, axis, axis=dim, tiled=True), 0, [])  12.4 us
  transfers between devices with their start and end apart: 4, of which 3 were waited for; matrix products, arithmetic and copies ran while one was open for 15% of the time, Pallas kernels for 0%

profile of v1, /device:TPU:24, one launch (start us, length us, event | category | flops | bytes accessed | tf_op | source)
XLA Modules:
  0.0 265.2 jit_solution(11983238386930630671)
XLA Ops:
  9.6 11.7 %all-reduce.1 = (f32[256]{0:T(256)S(1)}, f32[256]{0:T(256)S(1)}, f32[256]{0:T(256)S(1)}) all-reduce(f32[256]{0:T(256)S(1)} %bitcast.459, f32[256]{0:T(256)S(1)} %bitcast.458, f32[256]{0:T(256)S(1)} %bitcast.457), channel_id=1, replica_groups=mesh['sp_0'=4,'sp_1'=4,'tp'=8] {'sp_0'}, use_global_device_ids=true, to_apply=%region_4.5 | all-reduce | flops 768 | bytes 6144 | tf_op jit(solution)/shard_map/psum | solution.py:19
  21.3 7.5 %all-reduce = (f32[256,1]{0,1:T(1,128)S(1)}, f32[256,1]{0,1:T(1,128)S(1)}, f32[256,1]{0,1:T(1,128)S(1)}) all-reduce(f32[256,1]{0,1:T(1,128)S(1)} %bitcast.460, f32[256,1]{0,1:T(1,128)S(1)} %bitcast.461, f32[256,1]{0,1:T(1,128)S(1)} %bitcast.462), channel_id=1, replica_groups=mesh['sp_0'=4,'sp_1'=4,'tp'=8] {'sp_1'}, use_global_device_ids=true, to_apply=%region_5.6 | all-reduce | flops 768 | bytes 6144 | tf_op jit(solution)/shard_map/psum | solution.py:19
  28.8 13.3 %all_gather.6 = f32[2048,3]{0,1:T(4,128)S(1)} all-gather(f32[256,3]{0,1:T(4,128)S(1)} %pad_maximum_fusion.4), channel_id=1, replica_groups=mesh['sp_0'=4,'sp_1'=4,'tp'=8] {'tp'}, dimensions={0}, use_global_device_ids=true | all-gather | bytes 27648 | tf_op jit(solution)/shard_map/all_gather | solution.py:26
  45.0 3.5 %stack.65 = bf16[8,192,2048]{2,1,0:T(8,128)(2,1)} broadcast(bf16[192,2048]{1,0:T(8,128)(2,1)S(1)} %fusion.16), dimensions={1,2} | broadcast | bytes 7077888 | tf_op jit(solution)/shard_map/stack | solution.py:162
  48.5 4.9 %all-to-all-start = ((bf16[8,192,2048]{2,1,0:T(8,128)(2,1)}), bf16[8,192,2048]{2,1,0:T(8,128)(2,1)}, u32[]{:S(2)}, u32[]{:S(2)}) async-start(bf16[8,192,2048]{2,1,0:T(8,128)(2,1)} %stack.65), calls=%async_computation | async-start | bytes 12582912 | tf_op jit(solution)/shard_map/all_to_all | solution.py:162
  61.5 5.6 %fusion.108 = f32[64,64,2,16,8]{1,3,4,2,0:T(8,128)} fusion(f32[64,64,2,15,1]{1,3,4,2,0:T(8,128)S(1)} %convolution_bitcast_fusion.16, s32[16,8]{0,1:T(8,128)S(1)} %copy.527), kind=kOutput, calls=%fused_computation.231 | convolution fusion | flops 188745600 | bytes 4686336 | tf_op jit(solution)/shard_map/nir,hrj,ckj->nhcik/dot_general | solution.py:96
  67.1 9.6 %copy.528 = f32[64,64,2,16,8]{0,1,2,3,4:T(8,128)} copy(f32[64,64,2,16,8]{1,3,4,2,0:T(8,128)} %fusion.108) | data formatting | bytes 8388608 | tf_op jit(solution)/shard_map/nir,hrj,ckj->nhcik/dot_general | solution.py:96
  76.9 3.8 %fusion.113 = f32[64,64,2,8,8]{1,4,3,2,0:T(8,128)} fusion(f32[64,64,2,15,1]{1,3,4,2,0:T(8,128)S(1)} %convolution_bitcast_fusion.16, s32[8,8]{1,0:T(8,128)S(1)} %gather_fusion.3), kind=kOutput, calls=%fused_computation.240 | convolution fusion | flops 94372800 | bytes 2588928 | tf_op jit(solution)/shard_map/nir,hrj,ckj->nhcik/dot_general | solution.py:96
  80.7 5.7 %copy.487 = f32[64,64,2,8,8]{0,1,2,3,4:T(8,128)} copy(f32[64,64,2,8,8]{1,4,3,2,0:T(8,128)} %fusion.113) | data formatting | bytes 4194304 | tf_op jit(solution)/shard_map/nir,hrj,ckj->nhcik/dot_general | solution.py:96
  86.4 12.4 %all-gather.2.cloned.1.call-done = bf16[1024,512]{1,0:T(8,128)(2,1)} async-done(((bf16[64,512]{1,0:T(8,128)(2,1)}), bf16[1024,512]{1,0:T(8,128)(2,1)}) %all-gather.2.cloned.1.call-update) | async-done | bytes 1048592 | tf_op jit(solution)/shard_map/all_gather | solution.py:38
  101.9 23.6 %all-to-all-done = bf16[8,192,2048]{2,1,0:T(8,128)(2,1)} async-done(((bf16[8,192,2048]{2,1,0:T(8,128)(2,1)}), bf16[8,192,2048]{2,1,0:T(8,128)(2,1)}, u32[]{:S(2)}, u32[]{:S(2)}) %all-to-all-start) | async-done | bytes 6291488 | tf_op jit(solution)/shard_map/all_to_all | solution.py:162
  125.5 4.6 %multiply_reduce_fusion = (f32[1536,2]{0,1:T(2,128)S(1)}, f32[1536,2,128]{0,2,1:T(8,128)S(1)}) fusion(bf16[1536,2048,1]{1,0,2:T(8,128)(2,1)} %bitcast.15, bf16[2,128,2048]{2,1,0:T(8,128)(2,1)S(1)} %bitcast.443), kind=kOutput, calls=%fused_computation.47 | convolution fusion | flops 1611396096 | bytes 8925184 | tf_op jit(solution)/shard_map/dot_general | solution.py:168
  130.2 4.6 %convolution_convert_fusion = bf16[1536,256]{0,1:T(8,128)(2,1)S(1)} fusion(bf16[1536,2048]{1,0:T(8,128)(2,1)} %bitcast.14, bf16[2048,256]{1,0:T(8,128)(2,1)S(1)} %copy-done), kind=kOutput, calls=%fused_computation.29 | convolution fusion | flops 1611005952 | bytes 8126464 | tf_op jit(solution)/shard_map/dot_general | solution.py:170
  139.8 7.5 %fusion.137 = (bf16[16,64,1,2,128]{4,3,2,1,0:T(2,128)(2,1)S(1)}, bf16[16,64,1,2,128]{4,3,2,1,0:T(2,128)(2,1)S(1)}, bf16[16,64,1,2,128]{4,3,2,1,0:T(2,128)(2,1)S(...) fusion(bf16[24,64,2,2,128]{4,3,2,1,0:T(2,128)(2,1)S(1)} %concat, ...), kind=kLoop, calls=%fused_computation.283 | loop fusion | bytes 16777216 | tf_op jit(solution)/shard_map/slice | solution.py:211
  147.3 16.5 %multiply_reduce_fusion.1 = (f32[1536,2]{0,1:T(2,128)S(1)}, f32[1536,2,128]{2,0,1:T(8,128)S(1)}) fusion(bf16[1536,2048,1]{1,0,2:T(8,128)(2,1)} %bitcast.15, bf16[2,128,2048]{2,1,0:T(8,128)(2,1)S(1)} %bitcast.442), kind=kOutput, calls=%fused_computation.49 | convolution fusion | flops 1611396096 | bytes 8925184 | tf_op jit(solution)/shard_map/dot_general | solution.py:165
  168.9 3.2 %copy-done.8 = f32[16,2,64,8,64]{2,4,1,0,3:T(8,128)} copy-done((f32[16,2,64,8,64]{2,4,1,0,3:T(8,128)}, f32[16,2,64,8,64]{2,4,1,0,3:T(8,128)S(1)}, u32[]{:S(2)}) %copy-start.8) | copy-done | bytes 4194328
  173.1 12.2 %fusion.133 = (f32[16,2,64]{2,1,0:T(2,128)S(1)}, f32[16,2,64,8,64]{2,4,1,0,3:T(8,128)}) fusion(f32[64,64,2,16,8]{0,1,2,3,4:T(8,128)} %copy.528, f32[16,2,64,8,64]{2,4,1,0,3:T(8,128)} %copy-done.8, pred[64,64]{0,1:T(8,128)(4,1)S(1)} %fusion.111), kind=kLoop, calls=%fused_computation.281 | loop fusion | flops 4192256 | bytes 12595200 | tf_op jit(solution)/shard_map/reduce_max | solution.py:118
  185.3 4.6 %fusion.3 = f32[16,2,64]{2,0,1:T(8,128)S(1)} fusion(f32[2,1024,16,64]{1,3,2,0:T(8,128)} %bitcast.418, f32[16,2,64]{2,0,1:T(8,128)S(1)} %copy_maximum_fusion, f32[2]{0:T(128)S(1)} %copy-done.25), kind=kLoop, calls=%fused_computation.14 | loop fusion | flops 8386560 | bytes 8405000 | tf_op jit(solution)/shard_map/reduce_sum | solution.py:121
  204.7 4.0 %collective-permute-start = (bf16[4,64,512]{2,1,0:T(8,128)(2,1)S(1)}, bf16[4,64,512]{2,1,0:T(8,128)(2,1)S(1)}, u32[]{:S(2)}, u32[]{:S(2)}) collective-permute-start(bf16[4,64,512]{2,1,0:T(8,128)(2,1)S(1)} %bitcast.452), channel_id=1, source_target_pairs={{0,8},{8,16},{16,24},{24,32},{32,40},{40,48},{48,56},{56,64},{64,7... | collective-permute-start | bytes 786440 | tf_op jit(solution)/shard_map/ppermute | solution.py:53
  216.1 4.3 %collective-permute-done.1 = bf16[4,64,512]{2,1,0:T(8,128)(2,1)S(1)} collective-permute-done((bf16[4,64,512]{2,1,0:T(8,128)(2,1)S(1)}, bf16[4,64,512]{2,1,0:T(8,128)(2,1)S(1)}, u32[]{:S(2)}, u32[]{:S(2)}) %collective-permute-start.1) | collective-permute-done | bytes 262176 | tf_op jit(solution)/shard_map/ppermute | solution.py:55
  222.1 3.0 %gather_fusion.2 = bf16[64,64,2,2,128]{4,1,3,2,0:T(8,128)(2,1)} fusion(bf16[32,64,2,2,128]{4,1,3,2,0:T(8,128)(2,1)S(1)} %pad_maximum_fusion, s32[1024]{0:T(1024)S(1)} %pad_clamp_fusion), kind=kCustom, calls=%fused_computation.2 | custom fusion | bytes 8388864 | tf_op jit(solution)/shard_map/jit(_take)/gather | solution.py:195
  225.2 2.6 copy_select_fusion
  239.5 15.7 %all_to_all.24 = bf16[8,192,256]{2,1,0:T(8,128)(2,1)S(1)} all-to-all(bf16[8,192,256]{2,1,0:T(8,128)(2,1)S(1)} %bitcast.436), channel_id=1, replica_groups=mesh['sp_0'=4,'sp_1'=4,'tp'=8] {'tp'}, dimensions={0} | all-to-all | bytes 1572864 | tf_op jit(solution)/shard_map/all_to_all | solution.py:221
  255.4 2.7 %fusion.10 = bf16[192,2048]{1,0:T(8,128)(2,1)} fusion(bf16[192,2048]{1,0:T(8,128)(2,1)S(1)} %bitcast.444, bf16[2048,2048]{1,0:T(8,128)(2,1)S(1)} %bitcast.464, bf16[192,2048]{1,0:T(8,128)(2,1)S(1)} %copy-done.12, f32[2048]{0:T(1024)S(1)} %bitcast.456), kind=kOutput, calls=%fused_computation.31 | convolution fusion | flops 1612185600 | bytes 10756096 | tf_op jit(solution)/shard_map/dot_general | solution.py:222
  (188 shorter events, 63.4 us)
Async XLA Ops:
  6.5 47.8 %copy-start = (bf16[2048,256]{1,0:T(8,128)(2,1)S(1)}, bf16[2048,256]{1,0:T(8,128)(2,1)}, u32[]{:S(2)}) copy-start(bf16[2048,256]{1,0:T(8,128)(2,1)} %param.25) | copy-start | bytes 3145732
  48.5 5.0 %copy-start.15 = (bf16[64,2048]{1,0:T(8,128)(2,1)S(1)}, bf16[64,2048]{1,0:T(8,128)(2,1)}, u32[]{:S(2)}) copy-start(bf16[64,2048]{1,0:T(8,128)(2,1)} %param.22) | copy-start | bytes 786436
  48.5 5.2 %copy-start.11 = (bf16[2048,256]{1,0:T(8,128)(2,1)S(1)}, bf16[2048,256]{1,0:T(8,128)(2,1)}, u32[]{:S(2)}) copy-start(bf16[2048,256]{1,0:T(8,128)(2,1)} %param.24) | copy-start | bytes 3145732
  48.5 5.2 %copy-start.23 = (f32[2048]{0:T(1024)S(1)}, f32[2048]{0:T(1024)}, u32[]{:S(2)}) copy-start(f32[2048]{0:T(1024)} %param.21) | copy-start | bytes 24580
  48.5 5.7 %copy-start.27 = (f32[128]{0:T(128)S(1)}, f32[128]{0:T(128)}, u32[]{:S(2)}) copy-start(f32[128]{0:T(128)} %param.27) | copy-start | bytes 1540
  48.5 7.0 %copy-start.24 = (f32[2,15,31]{2,0,1:T(2,128)S(1)}, f32[2,15,31]{2,0,1:T(2,128)}, u32[]{:S(2)}) copy-start(f32[2,15,31]{2,0,1:T(2,128)} %param.28) | copy-start | bytes 11164
  48.5 77.0 %all-to-all-start = ((bf16[8,192,2048]{2,1,0:T(8,128)(2,1)}), bf16[8,192,2048]{2,1,0:T(8,128)(2,1)}, u32[]{:S(2)}, u32[]{:S(2)}) async-start(bf16[8,192,2048]{2,1,0:T(8,128)(2,1)} %stack.65), calls=%async_computation | async-start | bytes 12582912 | tf_op jit(solution)/shard_map/all_to_all | solution.py:162
  53.4 45.4 %all-gather.2.cloned.1.call-start = ((), (), s32[]{:S(2)}) async-start(), calls=%async_computation.2 | async-start | bytes 1114112 | tf_op jit(solution)/shard_map/all_gather | solution.py:38
  80.7 44.8 %copy-start.20 = (bf16[256,2048]{1,0:T(8,128)(2,1)S(1)}, bf16[256,2048]{1,0:T(8,128)(2,1)}, u32[]{:S(2)}) copy-start(bf16[256,2048]{1,0:T(8,128)(2,1)} %copy.578) | copy-start | bytes 3145732
  139.8 7.5 %copy-start.19 = (bf16[256,2048]{1,0:T(8,128)(2,1)S(1)}, bf16[256,2048]{1,0:T(8,128)(2,1)}, u32[]{:S(2)}) copy-start(bf16[256,2048]{1,0:T(8,128)(2,1)} %copy.577) | copy-start | bytes 3145732
  147.2 16.6 %copy-start.28 = (f32[128]{0:T(128)S(1)}, f32[128]{0:T(128)}, u32[]{:S(2)}) copy-start(f32[128]{0:T(128)} %param.26) | copy-start | bytes 1540
  147.2 17.1 %copy-start.10 = (bf16[128,2,8,128]{3,2,1,0:T(8,128)(2,1)S(1)}, bf16[128,2,8,128]{3,2,1,0:T(8,128)(2,1)}, u32[]{:S(2)}) copy-start(bf16[128,2,8,128]{3,2,1,0:T(8,128)(2,1)} %get-tuple-element.58) | copy-start | bytes 1572868
  165.6 6.5 %copy-start.3 = (f32[2,1024,1024]{1,2,0}, f32[2,1024,1024]{1,2,0:S(1)}, u32[]{:S(2)}) copy-start(f32[2,1024,1024]{1,2,0:S(1)} %fusion.58) | copy-start | bytes 25165828
  167.3 4.9 %copy-start.25 = (f32[2]{0:T(128)S(1)}, f32[2]{0:T(128)}, u32[]{:S(2)}) copy-start(f32[2]{0:T(128)} %param.29) | copy-start | bytes 28
  168.9 3.2 %copy-start.8 = (f32[16,2,64,8,64]{2,4,1,0,3:T(8,128)}, f32[16,2,64,8,64]{2,4,1,0,3:T(8,128)S(1)}, u32[]{:S(2)}) copy-start(f32[16,2,64,8,64]{2,4,1,0,3:T(8,128)S(1)} %fusion.26) | copy-start | bytes 12582916
  185.3 6.2 %copy-start.14 = (bf16[1536,256]{0,1:T(8,128)(2,1)S(1)}, bf16[1536,256]{0,1:T(8,128)(2,1)}, u32[]{:S(2)}) copy-start(bf16[1536,256]{0,1:T(8,128)(2,1)} %copy-done.13) | copy-start | bytes 2359300
  185.3 6.3 %copy-start.2 = (f32[16,2,64,8,64]{2,4,1,0,3:T(8,128)S(1)}, f32[16,2,64,8,64]{2,4,1,0,3:T(8,128)}, u32[]{:S(2)}) copy-start(f32[16,2,64,8,64]{2,4,1,0,3:T(8,128)} %get-tuple-element.12) | copy-start | bytes 12582916
  194.6 3.4 %copy-start.4 = (f32[2,1024,1024]{1,2,0:S(1)}, f32[2,1024,1024]{1,2,0}, u32[]{:S(2)}) copy-start(f32[2,1024,1024]{1,2,0} %copy-done.3) | copy-start | bytes 25165828
  204.7 11.3 %collective-permute-start = (bf16[4,64,512]{2,1,0:T(8,128)(2,1)S(1)}, bf16[4,64,512]{2,1,0:T(8,128)(2,1)S(1)}, u32[]{:S(2)}, u32[]{:S(2)}) collective-permute-start(bf16[4,64,512]{2,1,0:T(8,128)(2,1)S(1)} %bitcast.452), channel_id=1, source_target_pairs={{0,8},{8,16},{16,24},{24,32},{32,40},{40,48},{48,56},{56,64},{64,7... | collective-permute-start | bytes 786440 | tf_op jit(solution)/shard_map/ppermute | solution.py:53
  208.8 11.5 %collective-permute-start.1 = (bf16[4,64,512]{2,1,0:T(8,128)(2,1)S(1)}, bf16[4,64,512]{2,1,0:T(8,128)(2,1)S(1)}, u32[]{:S(2)}, u32[]{:S(2)}) collective-permute-start(bf16[4,64,512]{2,1,0:T(8,128)(2,1)S(1)} %bitcast.451), channel_id=1, source_target_pairs={{8,0},{16,8},{24,16},{32,24},{40,32},{48,40},{56,48},{64,56},{72,6... | collective-permute-start | bytes 786440 | tf_op jit(solution)/shard_map/ppermute | solution.py:55
  236.4 18.9 %slice-start = ((s8[8388608]{0:T(1024)(128)(4,1)}), s8[4194304]{0:T(1024)(128)(4,1)S(1)}, s32[]{:S(2)}) async-start(s8[8388608]{0:T(1024)(128)(4,1)} %bitcast.463), calls=%async_computation.3 | async-start | bytes 8388608
  238.3 17.0 %slice-start.1 = ((s8[8388608]{0:T(1024)(128)(4,1)}), s8[4194304]{0:T(1024)(128)(4,1)S(1)}, s32[]{:S(2)}) async-start(s8[8388608]{0:T(1024)(128)(4,1)} %bitcast.463), calls=%async_computation.4 | async-start | bytes 8388608
  239.1 16.3 %copy-start.12 = (bf16[192,2048]{1,0:T(8,128)(2,1)S(1)}, bf16[192,2048]{1,0:T(8,128)(2,1)}, u32[]{:S(2)}) copy-start(bf16[192,2048]{1,0:T(8,128)(2,1)} %param.16) | copy-start | bytes 2359300
  255.3 2.7 %copy-start.1 = (bf16[2048,256]{1,0:T(8,128)(2,1)S(1)}, bf16[2048,256]{1,0:T(8,128)(2,1)}, u32[]{:S(2)}) copy-start(bf16[2048,256]{1,0:T(8,128)(2,1)} %param.25) | copy-start | bytes 3145732
  (11 other events, 21.9 us)
Sparse Core Ops, SparseCore 0:
  56.3 42.3 all-gather.1
